TPU v7x, 32 devices: a whole 2x2x4 slice. The times are simulated.
32 devices in a mesh: ep: 8 (over z, x), tp: 4 (over y, core).
Axes of the slice: x: 2, y: 2, z: 4, core: 2. Of those that a mesh axis runs over, the one named last changes fastest.
Arguments:
- queries: bfloat16 [2048, 1024], P('ep', 'tp'), may hold values from -6 to 6
- keys: bfloat16 [2048, 256], P('ep', 'tp'), may hold values from -6 to 6
- values: bfloat16 [2048, 256], P('ep', 'tp'), may hold values from -6 to 6
- q_gain: float32 [64], replicated, may hold values from 1 to 6
- k_gain: float32 [64], replicated, may hold values from 1 to 6
- out_weight: bfloat16 [1024, 2048], P('tp'), may hold values from -0.1875 to 0.1875
- tokens: bfloat16 [1024, 2048], P(('ep', 'tp')), may hold values from -6 to 6
- ffn_gain: float32 [2048], replicated, may hold values from 0.1 to 1.9
- route: int32 [1024, 2], P(('ep', 'tp')), may hold values from 0 to 7, all different within a row; in each aligned block of 32 rows (0 to 31, 32 to 63, ...) at most 16 rows name the same one
- route_weight: float32 [1024, 2], P(('ep', 'tp')), may hold values from 0.1 to 1
- gate_weight: bfloat16 [8, 2048, 3584], P('ep', None, 'tp'), may hold values from -0.125 to 0.125
- up_weight: bfloat16 [8, 2048, 3584], P('ep', None, 'tp'), may hold values from -0.125 to 0.125
- down_weight: bfloat16 [8, 3584, 2048], P('ep', 'tp'), may hold values from -0.09375 to 0.09375
Outputs:
- mixer_out: bfloat16 [2048, 2048], P(('ep', 'tp'))
- mixed: bfloat16 [1024, 2048], P(('ep', 'tp'))
Inputs may be any that keep to these rules, and one draw needn't show every extreme that they name: `route`: each row names 2 different experts. In every device's aligned block of 32 rows no expert is named more than 16 times, and in some blocks some expert is named exactly 16 times.
All inputs are finite; a program needn't handle non-finite values.
Results may differ from a plain program's by a relative error of at most 0.013.
The roundings to bfloat16 on the way count: a program that leaves them out, or rounds other values in their place, can miss the bound.
Values may be sent and summed in bfloat16 or wider, within the bound.
No kernel may reach another device: no remote copies, remote signals or barrier semaphores. Data moves between devices by JAX's collectives and lax.ppermute only.
A program may use at most 192 MiB of HBM per device.

v0:
```python
import jax
import jax.numpy as jnp
from jax import lax
from jax.sharding import PartitionSpec as P

GRID_W = 64
EPS = 1e-06
THETA = 10000.0


def head_norm(vals, gain):
    vals = vals.astype(jnp.float32)
    return vals * lax.rsqrt(jnp.mean(vals * vals, axis=-1, keepdims=True) + EPS) * gain


def rotate(vals, positions):
    pairs = vals.shape[-1] // 2
    quarter = pairs // 2
    freqs = THETA ** (-jnp.arange(quarter, dtype=jnp.float32) / quarter)
    grid_row = (positions // GRID_W).astype(jnp.float32)
    grid_col = (positions % GRID_W).astype(jnp.float32)
    angle = jnp.concatenate([grid_row[:, None] * freqs, grid_col[:, None] * freqs], axis=-1)
    cosine = jnp.cos(angle)[:, None, :]
    sine = jnp.sin(angle)[:, None, :]
    split = vals.reshape(vals.shape[:-1] + (pairs, 2))
    first = split[..., 0]
    second = split[..., 1]
    turned = jnp.stack([first * cosine - second * sine, first * sine + second * cosine], axis=-1)
    return turned.reshape(vals.shape)


def local(
    queries,
    keys,
    values,
    q_gain,
    k_gain,
    out_weight,
    tokens,
    ffn_gain,
    route,
    route_weight,
    gate_weight,
    up_weight,
    down_weight,
):
    local_rows = queries.shape[0]
    head_size = q_gain.shape[0]
    query_heads = queries.shape[1] // head_size
    key_heads = keys.shape[1] // head_size
    group = query_heads // key_heads
    key_width = key_heads * head_size
    positions = lax.axis_index("ep") * local_rows + jnp.arange(local_rows, dtype=jnp.int32)
    rot_q = rotate(
        head_norm(queries.reshape(local_rows, query_heads, head_size), q_gain), positions
    ).astype(jnp.bfloat16)
    rot_q = rot_q.reshape(local_rows, key_heads, group, head_size)
    rot_k = rotate(
        head_norm(keys.reshape(local_rows, key_heads, head_size), k_gain), positions
    ).astype(jnp.bfloat16)
    joined = jnp.concatenate([rot_k.reshape(local_rows, key_width), values], axis=1)
    scale = head_size ** (-0.5)

    def fold_block(carry, block):
        highest, denom, numer = carry
        key_block = block[:, :key_width].reshape(-1, key_heads, head_size)
        value_block = block[:, key_width:].reshape(-1, key_heads, head_size)
        scores = (
            jnp.einsum("qkgd,skd->qkgs", rot_q, key_block, preferred_element_type=jnp.float32)
            * scale
        )
        new_high = jnp.maximum(highest, jnp.max(scores, axis=-1))
        shrink = jnp.exp(highest - new_high)
        expo = jnp.exp(scores - new_high[..., None])
        denom = denom * shrink + jnp.sum(expo, axis=-1)
        numer = numer * shrink[..., None] + jnp.einsum(
            "qkgs,skd->qkgd",
            expo.astype(jnp.bfloat16),
            value_block,
            preferred_element_type=jnp.float32,
        )
        return ((new_high, denom, numer), None)

    start_high = jnp.full((local_rows, key_heads, group), -1e30, jnp.float32)
    start_denom = jnp.zeros((local_rows, key_heads, group), jnp.float32)
    start_numer = jnp.zeros((local_rows, key_heads, group, head_size), jnp.float32)
    carry = (start_high, start_denom, start_numer)
    piece = lax.all_gather(joined, "ep", axis=0, tiled=True)
    length = piece.shape[0]
    size = length
    while size > 2048 and size % 2 == 0:
        size = size // 2
    blocks = piece.reshape(length // size, size, piece.shape[1])
    carry, _ = lax.scan(fold_block, carry, blocks)
    highest, denom, numer = carry
    attended = (
        (numer / denom[..., None]).astype(jnp.bfloat16).reshape(local_rows, query_heads * head_size)
    )
    own_rows = tokens.shape[0]
    width = tokens.shape[1]
    picks_row = route.shape[1]
    experts = lax.axis_size("ep")
    capacity = 2 * own_rows * picks_row // experts
    token_float = tokens.astype(jnp.float32)
    normed = (
        token_float
        * lax.rsqrt(jnp.mean(token_float * token_float, axis=-1, keepdims=True) + EPS)
        * ffn_gain
    ).astype(jnp.bfloat16)
    flat_route = route.reshape(-1)
    expert_hot = (flat_route[:, None] == jnp.arange(experts, dtype=jnp.int32)[None, :]).astype(
        jnp.int32
    )
    earlier = jnp.cumsum(expert_hot, axis=0) - expert_hot
    rank = jnp.sum(earlier * expert_hot, axis=1)
    slot = flat_route * capacity + rank
    pick_hot = (slot[:, None] == jnp.arange(experts * capacity, dtype=jnp.int32)[None, :]).astype(
        jnp.bfloat16
    )
    row_hot = jnp.sum(pick_hot.reshape(own_rows, picks_row, experts * capacity), axis=1)
    outgoing = jnp.einsum("rs,rd->sd", row_hot, normed, preferred_element_type=jnp.float32).astype(
        jnp.bfloat16
    )
    outgoing = outgoing.reshape(experts, capacity, width)
    gate_local = gate_weight[0]
    up_local = up_weight[0]
    down_local = down_weight[0]
    arrived = lax.all_to_all(outgoing, "ep", split_axis=0, concat_axis=0, tiled=True)
    sources = arrived.shape[0]
    items = arrived.shape[1]
    slot_rows = arrived.reshape(sources * items, width)
    piece = lax.all_gather(slot_rows, "tp", axis=0, tiled=True)
    gate = jnp.dot(piece, gate_local, preferred_element_type=jnp.float32)
    upper = jnp.dot(piece, up_local, preferred_element_type=jnp.float32)
    hidden = (jax.nn.silu(gate) * upper).astype(jnp.bfloat16)
    worked = jnp.dot(hidden, down_local, preferred_element_type=jnp.float32).reshape(
        -1, items, width
    )
    head_partial = jnp.dot(attended, out_weight, preferred_element_type=jnp.float32)
    mixer_sum, expert_sum = (
        lax.psum_scatter(
            head_partial.astype(jnp.bfloat16), "tp", scatter_dimension=0, tiled=True
        ).astype(jnp.float32),
        lax.psum_scatter(worked.astype(jnp.bfloat16), "tp", scatter_dimension=0, tiled=True).astype(
            jnp.float32
        ),
    )
    mixer_out = mixer_sum.astype(jnp.bfloat16)
    home = expert_sum.astype(jnp.bfloat16)
    back = lax.all_to_all(home, "ep", split_axis=0, concat_axis=0, tiled=True)
    copies = jnp.dot(
        pick_hot, back.reshape(experts * capacity, width), preferred_element_type=jnp.float32
    )
    weighted = route_weight[..., None] * copies.reshape(own_rows, picks_row, width)
    mixed = jnp.sum(weighted, axis=1).astype(jnp.bfloat16)
    return (mixer_out, mixed)


def solution(mesh):
    placed = (
        P("ep", "tp"),
        P("ep", "tp"),
        P("ep", "tp"),
        P(),
        P(),
        P("tp", None),
        P(("ep", "tp"), None),
        P(),
        P(("ep", "tp"), None),
        P(("ep", "tp"), None),
        P("ep", None, "tp"),
        P("ep", None, "tp"),
        P("ep", "tp", None),
    )
    return jax.shard_map(
        local,
        mesh=mesh,
        in_specs=placed,
        out_specs=(P(("ep", "tp"), None), P(("ep", "tp"), None)),
        check_vma=False,
    )
```

profile of v0, /device:TPU:0, one launch (start us, length us, event | category | flops | bytes accessed | tf_op | source)
XLA Modules:
  0.0 136.9 jit_solution(23721503916896512)
XLA Ops:
  7.2 0.8 copy.46
  8.1 0.1 eq.54
  8.2 0.1 reduce_window_sum.11
  8.3 0.2 select_reduce_fusion
  8.5 0.1 reduce_sum.73
  8.6 0.1 copy.47
  8.7 0.7 multiply_add_fusion
  9.4 0.1 fusion.47
  9.5 1.0 fusion.30
  10.5 1.3 convolution_convert_fusion.1
  11.8 21.7 %all_to_all.10 = bf16[8,16,2048]{2,1,0:T(8,128)(2,1)} all-to-all(bf16[8,16,2048]{2,1,0:T(8,128)(2,1)S(1)} %bitcast.99), channel_id=1, replica_groups=mesh['ep'=8,'tp'=4] {'ep'}, dimensions={0} | all-to-all | bytes 1048576 | tf_op jit(solution)/shard_map/all_to_all | solution.py:128
  33.6 1.0 copy.44
  34.6 0.1 reshape.448
  34.7 0.8 mul.273
  35.6 0.2 multiply_multiply_fusion
  35.8 19.5 %all-gather.2.cloned.1.call-done = bf16[512,2048]{1,0:T(8,128)(2,1)} async-done(((bf16[128,2048]{1,0:T(8,128)(2,1)}), bf16[512,2048]{1,0:T(8,128)(2,1)}) %all-gather.2.cloned.1.call-update) | async-done | bytes 2097168 | tf_op jit(solution)/shard_map/all_gather | solution.py:132
  55.3 5.1 %fusion.10 = f32[512,896]{1,0:T(8,128)S(1)} fusion(bf16[512,2048]{1,0:T(8,128)(2,1)} %all-gather.2.cloned.1.call-done, bf16[1,2048,896]{2,1,0:T(8,128)(2,1)} %param.23), kind=kOutput, calls=%fused_computation.11 | convolution fusion | flops 1879048192 | bytes 7602176 | tf_op jit(solution)/shard_map/dot_general | solution.py:133
  60.5 2.4 %multiply_convert_fusion = bf16[512,896]{1,0:T(8,128)(2,1)S(1)} fusion(f32[512,896]{1,0:T(8,128)S(1)} %fusion.10, bf16[512,2048]{1,0:T(8,128)(2,1)S(1)} %copy-done.7, bf16[1,2048,896]{2,1,0:T(8,128)(2,1)S(1)} %copy-done.5), kind=kOutput, calls=%fused_computation.17 | convolution fusion | flops 1881800704 | bytes 8519680 | tf_op jit(solution)/shard_map/dot_general | solution.py:134
  62.9 3.7 %fusion.12 = bf16[32,16,2048]{2,1,0:T(8,128)(2,1)} fusion(bf16[32,16,896]{2,1,0:T(8,128)(2,1)S(1)} %bitcast.101, bf16[1,896,2048]{2,1,0:T(8,128)(2,1)S(1)} %copy-done.6), kind=kOutput, calls=%fused_computation.13 | convolution fusion | flops 1880096768 | bytes 6684672 | tf_op jit(solution)/shard_map/dot_general | solution.py:136
  66.8 0.1 fusion.44
  66.9 0.3 subtract_convert_fusion
  67.3 0.3 pad_maximum_fusion
  67.7 0.1 fusion.38
  67.8 0.1 subtract_convert_fusion.1
  68.1 31.6 %all_gather.6 = bf16[2048,128]{0,1:T(8,128)(2,1)S(1)} all-gather(bf16[256,128]{0,1:T(8,128)(2,1)S(1)} %pad_maximum_fusion.1), channel_id=1, replica_groups=mesh['ep'=8,'tp'=4] {'ep'}, dimensions={0}, use_global_device_ids=true | all-gather | bytes 589824 | tf_op jit(solution)/shard_map/all_gather | solution.py:88
  99.7 1.3 bitcast_reduce_fusion
  101.0 1.4 %fusion.1 = f32[256,4]{0,1:T(4,128)S(1)} fusion(f32[2048,256,4]{1,0,2:T(8,128)S(1)} %get-tuple-element.37, f32[256,4]{0,1:T(4,128)S(1)} %broadcast_maximum_fusion), kind=kLoop, calls=%fused_computation.3 | loop fusion | flops 6290432 | bytes 8396800 | tf_op jit(solution)/shard_map/while/body/eval_jaxpr/reduce_sum | solution.py:75
  102.4 1.5 %fusion.27 = bf16[1,64,256,4]{2,1,3,0:T(8,128)(2,1)S(1)} fusion(f32[2048,256,4]{1,0,2:T(8,128)S(1)} %get-tuple-element.37, f32[256,4]{0,1:T(4,128)S(1)} %broadcast_maximum_fusion, bf16[2048,128]{0,1:T(8,128)(2,1)S(1)} %all_gather.6, f32[256,4]{0,1:T(4,128)S(1)} %get-tuple-element.29, f32[256,4]{0,1:T(4,128)S(1)} %get-tuple-element.28), kind=kOutput, calls=%fused_computation.22 | convolution fusion | flops 274923520 | bytes 8794112 | tf_op jit(solution)/shard_map/while/body/eval_jaxpr/qkgs,skd->qkgd/dot_general | solution.py:76
  104.0 1.4 %convolution_convert_fusion = bf16[256,2048]{1,0:T(8,128)(2,1)} fusion(bf16[256,256]{0,1:T(8,128)(2,1)S(1)} %bitcast.100, bf16[256,2048]{1,0:T(8,128)(2,1)S(1)} %copy-done), kind=kOutput, calls=%fused_computation.14 | convolution fusion | flops 268959744 | bytes 2228224 | tf_op jit(solution)/shard_map/dot_general | solution.py:139
  105.5 15.8 %all_to_all.11 = bf16[8,16,2048]{2,1,0:T(8,128)(2,1)S(1)} all-to-all(bf16[8,16,2048]{2,1,0:T(8,128)(2,1)} %reduce-scatter.5.cloned.1.call-done), channel_id=1, replica_groups=mesh['ep'=8,'tp'=4] {'ep'}, dimensions={0} | all-to-all | bytes 1048576 | tf_op jit(solution)/shard_map/all_to_all | solution.py:150
  121.3 0.9 fusion.17
  122.2 8.1 %reduce-scatter.3.cloned.1.call-done = bf16[64,2048]{1,0:T(8,128)(2,1)} async-done(((bf16[256,2048]{1,0:T(8,128)(2,1)}), bf16[64,2048]{1,0:T(8,128)(2,1)}) %reduce-scatter.3.cloned.1.call-update) | async-done | bytes 262160 | tf_op jit(solution)/shard_map/reduce_scatter | solution.py:141
  (41 shorter events, 0.7 us)
Async XLA Ops:
  7.2 96.8 %copy-start = (bf16[256,2048]{1,0:T(8,128)(2,1)S(1)}, bf16[256,2048]{1,0:T(8,128)(2,1)}, u32[]{:S(2)}) copy-start(bf16[256,2048]{1,0:T(8,128)(2,1)} %param.18) | copy-start | bytes 3145732
  7.2 48.1 %all-gather.2.cloned.1.call-start = ((), (), s32[]{:S(2)}) async-start(), calls=%async_computation.5 | async-start | bytes 2621440 | tf_op jit(solution)/shard_map/all_gather | solution.py:132
  33.5 71.9 %reduce-scatter.5.cloned.1.call-start = ((), (), s32[]{:S(2)}) async-start(), calls=%async_computation.6 | async-start | bytes 2621440 | tf_op jit(solution)/shard_map/reduce_scatter | solution.py:144
  55.3 5.2 %copy-start.5 = (bf16[1,2048,896]{2,1,0:T(8,128)(2,1)S(1)}, bf16[1,2048,896]{2,1,0:T(8,128)(2,1)}, u32[]{:S(2)}) copy-start(bf16[1,2048,896]{2,1,0:T(8,128)(2,1)} %param.24) | copy-start | bytes 11010052
  55.3 5.2 %copy-start.7 = (bf16[512,2048]{1,0:T(8,128)(2,1)S(1)}, bf16[512,2048]{1,0:T(8,128)(2,1)}, u32[]{:S(2)}) copy-start(bf16[512,2048]{1,0:T(8,128)(2,1)} %all-gather.2.cloned.1.call-done) | copy-start | bytes 6291460
  60.5 2.4 %copy-start.6 = (bf16[1,896,2048]{2,1,0:T(8,128)(2,1)S(1)}, bf16[1,896,2048]{2,1,0:T(8,128)(2,1)}, u32[]{:S(2)}) copy-start(bf16[1,896,2048]{2,1,0:T(8,128)(2,1)} %param.25) | copy-start | bytes 11010052
  62.9 4.7 %copy-start.1 = (bf16[256,64]{0,1:T(8,128)(2,1)S(1)}, bf16[256,64]{0,1:T(8,128)(2,1)}, u32[]{:S(2)}) copy-start(bf16[256,64]{0,1:T(8,128)(2,1)} %param.14) | copy-start | bytes 98308
  62.9 4.7 %copy-start.4 = (f32[64]{0:T(128)S(1)}, f32[64]{0:T(128)}, u32[]{:S(2)}) copy-start(f32[64]{0:T(128)} %param.17) | copy-start | bytes 772
  66.6 1.5 %copy-start.2 = (bf16[256,64]{0,1:T(8,128)(2,1)S(1)}, bf16[256,64]{0,1:T(8,128)(2,1)}, u32[]{:S(2)}) copy-start(bf16[256,64]{0,1:T(8,128)(2,1)} %param.15) | copy-start | bytes 98308
  66.6 63.7 %reduce-scatter.3.cloned.1.call-start = ((), (), s32[]{:S(2)}) async-start(), calls=%async_computation.4 | async-start | bytes 1310720 | tf_op jit(solution)/shard_map/reduce_scatter | solution.py:141
  103.9 17.3 %copy-start.3 = (f32[32,2]{0,1:T(2,128)S(1)}, f32[32,2]{0,1:T(2,128)}, u32[]{:S(2)}) copy-start(f32[32,2]{0,1:T(2,128)} %param.22) | copy-start | bytes 772
Sparse Core Ops, SparseCore 0:
  33.7 21.5 all-gather.1
  66.8 31.1 reduce-scatter.4
  105.6 24.7 reduce-scatter.2
where the time goes:
time: 137 us
  blocking collectives  69.1 us (50%)
  waiting for transfers between devices  27.7 us (20%)
  matrix products  17.7 us (13%)
  between operations  14 us (10%)
  other arithmetic  4.93 us (4%)
  local copies, waits for them, and re-layouts  3.26 us (2%)
    all_gather x1, blocking collectives, local(): piece = lax.all_gather(joined, 'ep', axis=0, tiled=True)  31.6 us
    all_to_all x1, blocking collectives, local(): lax.all_to_all(outgoing, 'ep', split_axis=0, concat_axis=0, tiled=True)  21.7 us
    all_gather x1, waiting for transfers between devices, local(): piece = lax.all_gather(slot_rows, 'tp', axis=0, tiled=True)  19.5 us
    all_to_all x1, blocking collectives, local(): back = lax.all_to_all(home, 'ep', split_axis=0, concat_axis=0, tiled=True)  15.8 us
    reduce_scatter x1, waiting for transfers between devices, local(): lax.psum_scatter(head_partial.astype(jnp.bfloat16), 'tp', scatter_dimensi...  8.13 us
    dot_general x1, matrix products, local(): gate = jnp.dot(piece, gate_local, preferred_element_type=jnp.float32)  5.14 us
    dot_general x1, matrix products, local(): jnp.dot(hidden, down_local, preferred_element_type=jnp.float32)  3.69 us
  transfers between devices with their start and end apart: 3, of which 2 were waited for; matrix products, arithmetic and copies ran while one was open for 7% of the time, Pallas kernels for 0%

commit v1 on v0

--- a/solution.py
+++ b/solution.py
@@ -85,7 +85,8 @@
     start_denom = jnp.zeros((local_rows, key_heads, group), jnp.float32)
     start_numer = jnp.zeros((local_rows, key_heads, group, head_size), jnp.float32)
     carry = (start_high, start_denom, start_numer)
-    piece = lax.all_gather(joined, "ep", axis=0, tiled=True)
+    copies_2 = jnp.concatenate([joined] * lax.axis_size("ep"), axis=0)
+    piece = lax.all_to_all(copies_2, "ep", 0, 0, tiled=True)
     length = piece.shape[0]
     size = length
     while size > 2048 and size % 2 == 0:

time: 137 us -> 133 us (0.971)
  blocking collectives: 69.1 us -> 41.6 us
  waiting for transfers between devices: 27.7 us -> 43.7 us
  starting transfers between devices: 0.12 us -> 5.81 us
  other arithmetic: 4.93 us -> 6.5 us
    all_gather x1 -> x0, blocking collectives: 31.6 us -> none  [local(): piece = lax.all_gather(joined, 'ep', axis=0, tiled=True)]
    all_to_all x0 -> x1, waiting for transfers between devices: none -> 13.2 us  [local(): piece = lax.all_to_all(copies_2, 'ep', 0, 0, tiled=True)]
    all_to_all x0 -> x1, starting transfers between devices: none -> 5.51 us  [local(): piece = lax.all_to_all(copies_2, 'ep', 0, 0, tiled=True)]
    all_to_all x1, blocking collectives: 15.8 us -> 19.9 us  [local(): back = lax.all_to_all(home, 'ep', split_axis=0, concat_axis=0, tiled=True)]
    reduce_scatter x1, waiting for transfers between devices: 0.02 us -> 3.73 us  [local(): lax.psum_scatter(worked.astype(jnp.bfloat16), 'tp', scatter_dimension=0,...]
  transfers between devices with their start and end apart: 3 -> 4, of which waited for: 2 -> 4; matrix products, arithmetic and copies ran while one was open for 7% -> 9% of each run, Pallas kernels for 0% -> 0%
where the time goes in v1:
time: 133 us; the launch traced here: 132 us
  waiting for transfers between devices  43.7 us (33%)
  blocking collectives  41.6 us (31%)
  matrix products  17.7 us (13%)
  between operations  14.1 us (11%)
  other arithmetic  6.5 us (5%)
  starting transfers between devices  5.81 us (4%)
  local copies, waits for them, and re-layouts  3.05 us (2%)
    all_to_all x1, blocking collectives, local(): lax.all_to_all(outgoing, 'ep', split_axis=0, concat_axis=0, tiled=True)  21.7 us
    all_to_all x1, blocking collectives, local(): back = lax.all_to_all(home, 'ep', split_axis=0, concat_axis=0, tiled=True)  19.9 us
    all_gather x1, waiting for transfers between devices, local(): piece = lax.all_gather(slot_rows, 'tp', axis=0, tiled=True)  19.6 us
    all_to_all x1, waiting for transfers between devices, local(): piece = lax.all_to_all(copies_2, 'ep', 0, 0, tiled=True)  13.2 us
    reduce_scatter x1, waiting for transfers between devices, local(): lax.psum_scatter(head_partial.astype(jnp.bfloat16), 'tp', scatter_dimensi...  7.13 us
    all_to_all x1, starting transfers between devices, local(): piece = lax.all_to_all(copies_2, 'ep', 0, 0, tiled=True)  5.51 us
    dot_general x1, matrix products, local(): gate = jnp.dot(piece, gate_local, preferred_element_type=jnp.float32)  5.14 us
    reduce_scatter x1, waiting for transfers between devices, local(): lax.psum_scatter(worked.astype(jnp.bfloat16), 'tp', scatter_dimension=0,...  3.73 us
  transfers between devices with their start and end apart: 4, of which 4 were waited for; matrix products, arithmetic and copies ran while one was open for 9% of the time, Pallas kernels for 0%

profile of v1, /device:TPU:0, one launch (start us, length us, event | category | flops | bytes accessed | tf_op | source)
XLA Modules:
  0.0 132.4 jit_solution(8977682408791138012)
XLA Ops:
  7.2 0.8 copy.94
  8.3 0.2 select_reduce_fusion
  8.5 0.1 reduce_sum.73
  8.7 0.7 multiply_add_fusion
  9.5 1.0 fusion.30
  10.5 1.3 convolution_convert_fusion.1
  11.8 21.7 %all_to_all.22 = bf16[8,16,2048]{2,1,0:T(8,128)(2,1)} all-to-all(bf16[8,16,2048]{2,1,0:T(8,128)(2,1)S(1)} %bitcast.105), channel_id=1, replica_groups=mesh['ep'=8,'tp'=4] {'ep'}, dimensions={0} | all-to-all | bytes 1048576 | tf_op jit(solution)/shard_map/all_to_all | solution.py:129
  33.6 0.8 fusion.37
  34.4 0.8 fusion.38
  35.4 0.1 subtract_convert_fusion.1
  35.7 19.6 %all-gather.2.cloned.1.call-done = bf16[512,2048]{1,0:T(8,128)(2,1)} async-done(((bf16[128,2048]{1,0:T(8,128)(2,1)}), bf16[512,2048]{1,0:T(8,128)(2,1)}) %all-gather.2.cloned.1.call-update) | async-done | bytes 2097168 | tf_op jit(solution)/shard_map/all_gather | solution.py:133
  55.3 5.1 %fusion.10 = f32[512,896]{1,0:T(8,128)S(1)} fusion(bf16[512,2048]{1,0:T(8,128)(2,1)} %all-gather.2.cloned.1.call-done, bf16[1,2048,896]{2,1,0:T(8,128)(2,1)} %param.23), kind=kOutput, calls=%fused_computation.11 | convolution fusion | flops 1879048192 | bytes 7602176 | tf_op jit(solution)/shard_map/dot_general | solution.py:134
  60.5 2.4 %multiply_convert_fusion = bf16[512,896]{1,0:T(8,128)(2,1)S(1)} fusion(f32[512,896]{1,0:T(8,128)S(1)} %fusion.10, bf16[512,2048]{1,0:T(8,128)(2,1)S(1)} %copy-done.7, bf16[1,2048,896]{2,1,0:T(8,128)(2,1)S(1)} %copy-done.5), kind=kOutput, calls=%fused_computation.17 | convolution fusion | flops 1881800704 | bytes 8519680 | tf_op jit(solution)/shard_map/dot_general | solution.py:135
  62.9 3.7 %fusion.12 = bf16[32,16,2048]{2,1,0:T(8,128)(2,1)} fusion(bf16[32,16,896]{2,1,0:T(8,128)(2,1)S(1)} %bitcast.108, bf16[1,896,2048]{2,1,0:T(8,128)(2,1)S(1)} %copy-done.6), kind=kOutput, calls=%fused_computation.13 | convolution fusion | flops 1880096768 | bytes 6684672 | tf_op jit(solution)/shard_map/dot_general | solution.py:137
  66.8 0.3 copy.89
  67.1 1.0 copy.90
  68.1 5.5 %all-to-all-start = ((bf16[8,256,128]{1,2,0:T(8,128)(2,1)}), bf16[8,256,128]{1,2,0:T(8,128)(2,1)S(1)}, u32[]{:S(2)}, u32[]{:S(2)}) async-start(bf16[8,256,128]{1,2,0:T(8,128)(2,1)} %copy.90), calls=%async_computation | async-start | bytes 1048576 | tf_op jit(solution)/shard_map/all_to_all | solution.py:89
  73.6 0.2 reduce-scatter.3.cloned.1.call-start
  73.9 0.1 reshape.450
  74.2 0.1 fusion.44
  74.4 0.2 multiply_multiply_fusion
  74.6 0.3 subtract_convert_fusion
  74.9 0.3 pad_maximum_fusion
  75.3 13.2 %all-to-all-done = bf16[8,256,128]{1,2,0:T(8,128)(2,1)S(1)} async-done(((bf16[8,256,128]{1,2,0:T(8,128)(2,1)}), bf16[8,256,128]{1,2,0:T(8,128)(2,1)S(1)}, u32[]{:S(2)}, u32[]{:S(2)}) %all-to-all-start) | async-done | bytes 524320 | tf_op jit(solution)/shard_map/all_to_all | solution.py:89
  88.5 1.3 bitcast_reduce_fusion
  89.8 1.4 %fusion.1 = f32[256,4]{0,1:T(4,128)S(1)} fusion(f32[2048,256,4]{1,0,2:T(8,128)S(1)} %get-tuple-element.37, f32[256,4]{0,1:T(4,128)S(1)} %broadcast_maximum_fusion), kind=kLoop, calls=%fused_computation.3 | loop fusion | flops 6290432 | bytes 8396800 | tf_op jit(solution)/shard_map/while/body/eval_jaxpr/reduce_sum | solution.py:75
  91.2 1.5 %fusion.27 = bf16[1,64,256,4]{2,1,3,0:T(8,128)(2,1)S(1)} fusion(f32[2048,256,4]{1,0,2:T(8,128)S(1)} %get-tuple-element.37, f32[256,4]{0,1:T(4,128)S(1)} %broadcast_maximum_fusion, bf16[2048,128]{0,1:T(8,128)(2,1)S(1)} %bitcast.101, f32[256,4]{0,1:T(4,128)S(1)} %get-tuple-element.29, f32[256,4]{0,1:T(4,128)S(1)} %get-tuple-element.28), kind=kOutput, calls=%fused_computation.22 | convolution fusion | flops 274923520 | bytes 8794112 | tf_op jit(solution)/shard_map/while/body/eval_jaxpr/qkgs,skd->qkgd/dot_general | solution.py:76
  92.8 1.4 %convolution_convert_fusion = bf16[256,2048]{1,0:T(8,128)(2,1)} fusion(bf16[256,256]{0,1:T(8,128)(2,1)S(1)} %bitcast.107, bf16[256,2048]{1,0:T(8,128)(2,1)S(1)} %copy-done), kind=kOutput, calls=%fused_computation.14 | convolution fusion | flops 268959744 | bytes 2228224 | tf_op jit(solution)/shard_map/dot_general | solution.py:140
  94.2 3.7 %reduce-scatter.5.cloned.1.call-done = bf16[8,16,2048]{2,1,0:T(8,128)(2,1)} async-done(((bf16[32,16,2048]{2,1,0:T(8,128)(2,1)}), bf16[8,16,2048]{2,1,0:T(8,128)(2,1)}) %reduce-scatter.5.cloned.1.call-update) | async-done | bytes 524304 | tf_op jit(solution)/shard_map/reduce_scatter | solution.py:145
  98.0 19.9 %all_to_all.23 = bf16[8,16,2048]{2,1,0:T(8,128)(2,1)S(1)} all-to-all(bf16[8,16,2048]{2,1,0:T(8,128)(2,1)} %reduce-scatter.5.cloned.1.call-done), channel_id=1, replica_groups=mesh['ep'=8,'tp'=4] {'ep'}, dimensions={0} | all-to-all | bytes 1048576 | tf_op jit(solution)/shard_map/all_to_all | solution.py:151
  117.8 0.9 fusion.17
  118.8 7.1 %reduce-scatter.3.cloned.1.call-done = bf16[64,2048]{1,0:T(8,128)(2,1)} async-done(((bf16[256,2048]{1,0:T(8,128)(2,1)}), bf16[64,2048]{1,0:T(8,128)(2,1)}) %reduce-scatter.3.cloned.1.call-update) | async-done | bytes 262160 | tf_op jit(solution)/shard_map/reduce_scatter | solution.py:142
  (52 shorter events, 1.3 us)
Async XLA Ops:
  7.2 85.6 %copy-start = (bf16[256,2048]{1,0:T(8,128)(2,1)S(1)}, bf16[256,2048]{1,0:T(8,128)(2,1)}, u32[]{:S(2)}) copy-start(bf16[256,2048]{1,0:T(8,128)(2,1)} %param.18) | copy-start | bytes 3145732
  7.2 48.1 %all-gather.2.cloned.1.call-start = ((), (), s32[]{:S(2)}) async-start(), calls=%async_computation.6 | async-start | bytes 2621440 | tf_op jit(solution)/shard_map/all_gather | solution.py:133
  33.5 64.4 %reduce-scatter.5.cloned.1.call-start = ((), (), s32[]{:S(2)}) async-start(), calls=%async_computation.7 | async-start | bytes 2621440 | tf_op jit(solution)/shard_map/reduce_scatter | solution.py:145
  55.3 5.2 %copy-start.5 = (bf16[1,2048,896]{2,1,0:T(8,128)(2,1)S(1)}, bf16[1,2048,896]{2,1,0:T(8,128)(2,1)}, u32[]{:S(2)}) copy-start(bf16[1,2048,896]{2,1,0:T(8,128)(2,1)} %param.24) | copy-start | bytes 11010052
  55.3 5.2 %copy-start.7 = (bf16[512,2048]{1,0:T(8,128)(2,1)S(1)}, bf16[512,2048]{1,0:T(8,128)(2,1)}, u32[]{:S(2)}) copy-start(bf16[512,2048]{1,0:T(8,128)(2,1)} %all-gather.2.cloned.1.call-done) | copy-start | bytes 6291460
  60.5 2.4 %copy-start.6 = (bf16[1,896,2048]{2,1,0:T(8,128)(2,1)S(1)}, bf16[1,896,2048]{2,1,0:T(8,128)(2,1)}, u32[]{:S(2)}) copy-start(bf16[1,896,2048]{2,1,0:T(8,128)(2,1)} %param.25) | copy-start | bytes 11010052
  62.9 3.7 %copy-start.1 = (bf16[256,64]{0,1:T(8,128)(2,1)S(1)}, bf16[256,64]{0,1:T(8,128)(2,1)}, u32[]{:S(2)}) copy-start(bf16[256,64]{0,1:T(8,128)(2,1)} %param.15) | copy-start | bytes 98308
  66.6 7.2 %copy-start.2 = (bf16[256,256]{1,0:T(8,128)(2,1)S(1)}, bf16[256,256]{1,0:T(8,128)(2,1)}, u32[]{:S(2)}) copy-start(bf16[256,256]{1,0:T(8,128)(2,1)} %param.13) | copy-start | bytes 393220
  66.6 7.5 %copy-start.4 = (f32[64]{0:T(128)S(1)}, f32[64]{0:T(128)}, u32[]{:S(2)}) copy-start(f32[64]{0:T(128)} %param.16) | copy-start | bytes 772
  68.1 20.4 %all-to-all-start = ((bf16[8,256,128]{1,2,0:T(8,128)(2,1)}), bf16[8,256,128]{1,2,0:T(8,128)(2,1)S(1)}, u32[]{:S(2)}, u32[]{:S(2)}) async-start(bf16[8,256,128]{1,2,0:T(8,128)(2,1)} %copy.90), calls=%async_computation | async-start | bytes 1048576 | tf_op jit(solution)/shard_map/all_to_all | solution.py:89
  73.6 52.3 %reduce-scatter.3.cloned.1.call-start = ((), (), s32[]{:S(2)}) async-start(), calls=%async_computation.5 | async-start | bytes 1310720 | tf_op jit(solution)/shard_map/reduce_scatter | solution.py:142
  92.8 25.1 %copy-start.3 = (f32[32,2]{0,1:T(2,128)S(1)}, f32[32,2]{0,1:T(2,128)}, u32[]{:S(2)}) copy-start(f32[32,2]{0,1:T(2,128)} %param.22) | copy-start | bytes 772
Sparse Core Ops, SparseCore 0:
  33.7 21.5 all-gather.1
  66.8 31.1 reduce-scatter.4
  101.1 24.7 reduce-scatter.2
